TPU v7x, 256 devices: a whole 4x4x8 slice. The times are simulated.
256 devices in a mesh: sp: 64 (over z, y, core), tp: 4 (over x).
Axes of the slice: x: 4, y: 4, z: 8, core: 2. Of those that a mesh axis runs over, the one named last changes fastest.
Arguments:
- layer_grad: bfloat16 [12288, 2048], P('sp'), may hold values from -16 to 16
- routes: int32 [12288, 2], P('sp'), may hold values from 0 to 63, as said below
- route_weight: float32 [12288, 2], P('sp'), may hold values from 0.1 to 0.9
- slot_tokens: bfloat16 [64, 576, 2048], P('sp'), may hold values from -6 to 6
- gate_proj: bfloat16 [64, 2048, 1024], P('sp', None, 'tp'), may hold values from -0.125 to 0.125
- up_proj: bfloat16 [64, 2048, 1024], P('sp', None, 'tp'), may hold values from -0.125 to 0.125
- down_proj: bfloat16 [64, 1024, 2048], P('sp', 'tp'), may hold values from -0.1875 to 0.1875
- out_proj: bfloat16 [2048, 1024], P(None, 'tp'), may hold values from -0.1875 to 0.1875
- queries: bfloat16 [12288, 512], P('sp', 'tp'), may hold values from -6 to 6
- keys: bfloat16 [12288, 512], P('sp', 'tp'), may hold values from -6 to 6
- values: bfloat16 [12288, 1024], P('sp', 'tp'), may hold values from -6 to 6
- fwd_decay: float32 [12288, 512], P('sp', 'tp'), may hold values from -2 to 0
- bwd_decay: float32 [12288, 512], P('sp', 'tp'), may hold values from -2 to 0
Outputs:
- gate_grad: bfloat16 [64, 2048, 1024], P('sp', None, 'tp')
- up_grad: bfloat16 [64, 2048, 1024], P('sp', None, 'tp')
- down_grad: bfloat16 [64, 1024, 2048], P('sp', 'tp')
- proj_grad: float32 [2048, 1024], P('sp', 'tp')
- query_grad: bfloat16 [12288, 512], P('sp', 'tp')
- key_grad: bfloat16 [12288, 512], P('sp', 'tp')
- value_grad: bfloat16 [12288, 1024], P('sp', 'tp')
Inputs may be any that keep to these rules, and one draw needn't show every extreme that they name: `routes`: each row names two different experts of one group of 8 consecutive experts. In every aligned block of 192 rows one expert is named by 9 rows or more.
All inputs are finite; a program needn't handle non-finite values.
Results may differ from a plain program's by a relative error of at most 0.015.
Values may be sent and summed in bfloat16 or wider, within the bound.
A program may use at most 128 MiB of HBM per device.

v0:
```python
import jax
import jax.numpy as jnp
from jax import lax
from jax.sharding import Mesh
from jax.sharding import PartitionSpec as P

KEY_CHANNELS = 64
DV = 128
BLOCK = 64
SP = ("sp_0", "sp_1", "sp_2")
EPSILON = 1e-06


def filled_with(array, identity):
    return jax.tree.map(
        lambda a, e: jnp.broadcast_to(jnp.asarray(e, a.dtype), a.shape), array, identity
    )


def all_in_one(array, axis):
    leaves = jax.tree.leaves(array)
    sequence = sorted(range(len(leaves)), key=lambda k: -leaves[k].size)
    width = (1, *leaves[sequence[0]].shape)[-1]
    lines = [
        jnp.pad(leaves[k].reshape(-1), (0, -leaves[k].size % width)).reshape(-1, width)
        for k in sequence
    ]
    both, at, found = (lax.all_gather(jnp.concatenate(lines), axis), 0, {})
    for k, line in zip(sequence, lines):
        slab = both[:, at : at + len(line)].reshape(len(both), -1)
        found[k] = slab[:, : leaves[k].size].reshape(-1, *leaves[k].shape)
        at += len(line)
    numbers = iter(range(len(leaves)))
    return jax.tree.map(lambda _: found[next(numbers)], array)


def once_a_type(array, axis):
    leaves, found = (jax.tree.leaves(array), {})
    for leading, a in enumerate(leaves):
        if leading not in found:
            alike = [k for k, b in enumerate(leaves) if b.dtype == a.dtype]
            got = (
                all_in_one([leaves[k] for k in alike], axis)
                if len(alike) > 1
                else [lax.all_gather(a, axis)]
            )
            for k, b in zip(alike, got):
                found[k] = b
    numbers = iter(range(len(leaves)))
    return jax.tree.map(lambda _: found[next(numbers)], array)


def carried_in(array, axes, combine, identity, reverse):
    before = start = filled_with(array, identity)
    total = array
    for axis in reversed(axes):
        devices, index = (lax.axis_size(axis), lax.axis_index(axis))
        pieces = once_a_type(total, axis)
        inside, total = (start, start)
        for k in reversed(range(devices)) if reverse else range(devices):
            passed = k > index if reverse else k < index
            total = combine(total, jax.tree.map(lambda part: part[k], pieces))
            inside = jax.tree.map(lambda new, old: jnp.where(passed, new, old), total, inside)
        before = combine(inside, before)
    return before


def copy_for_each(array, axis):
    devices = lax.axis_size(axis)
    return lax.all_to_all(
        jnp.broadcast_to(array[None], (devices, *array.shape)), axis, 0, 0, tiled=True
    )


def in_order(pieces, dim):
    shape = list(pieces.shape[1:])
    shape[dim] *= pieces.shape[0]
    return jnp.moveaxis(pieces, 0, dim).reshape(shape)


def gathered_copies(array, axis, dim):
    pieces = copy_for_each(array, axis)
    return in_order(pieces, dim)


def split_up(array, dim, devices):
    before, after = (array.shape[:dim], array.shape[dim + 1 :])
    return jnp.moveaxis(array.reshape(*before, devices, -1, *after), dim, 0)


def sum_at_owner(array, axis, dim):
    pieces = split_up(array, dim, lax.axis_size(axis))
    arrived = lax.all_to_all(pieces, axis, split_axis=0, concat_axis=0, tiled=True)
    return arrived.sum(axis=0)


def sweep(query_rows, keyrows, valrows, log_decay, strict):
    nheads, length, kwidth = query_rows.shape
    vwidth = valrows.shape[-1]
    number = length // BLOCK
    offset = -1 if strict else 0
    causal = jnp.tril(jnp.ones((BLOCK, BLOCK), jnp.float32), offset)

    def split(array):
        return jnp.moveaxis(array.reshape(nheads, number, BLOCK, array.shape[-1]), 1, 0)

    def advance(carried_state, pieces):
        query_block, key_block, value_block, gblock = pieces
        running_total = jnp.cumsum(gblock, axis=1)
        middle = running_total[:, BLOCK // 2 - 1 : BLOCK // 2, :]
        scores = (
            jnp.einsum(
                "hik,hjk->hij",
                query_block * jnp.exp(running_total - middle),
                key_block * jnp.exp(middle - running_total),
            )
            * causal
        )
        inner = jnp.einsum("hij,hjv->hiv", scores, value_block)
        outer_product = jnp.einsum(
            "zuw,zwo->zuo", query_block * jnp.exp(running_total), carried_state
        )
        final_row = running_total[:, -1:, :]
        fresh_state = jnp.einsum(
            "xor,xot->xrt", key_block * jnp.exp(final_row - running_total), value_block
        )
        return (
            jnp.exp(final_row[:, 0, :])[:, :, None] * carried_state + fresh_state,
            inner + outer_product,
        )

    start_state = jnp.zeros((nheads, kwidth, vwidth), jnp.float32)
    final, outputs = lax.scan(
        advance, start_state, (split(query_rows), split(keyrows), split(valrows), split(log_decay))
    )
    return (jnp.moveaxis(outputs, 0, 1).reshape(nheads, length, vwidth), final)


def slot_ranks(expert_ids, experts):
    members = (expert_ids[:, None] == jnp.arange(experts, dtype=jnp.int32)[None, :]).astype(
        jnp.int32
    )
    before = jnp.cumsum(members, axis=0) - members
    return jnp.sum(before * members, axis=1)


def local_pass(query_rows, keyrows, valrows, fwd_log, bwd_log):
    forward_out, forward_end = sweep(query_rows, keyrows, valrows, fwd_log, False)
    backward_out, backward_end = sweep(
        jnp.flip(query_rows, 1),
        jnp.flip(keyrows, 1),
        jnp.flip(valrows, 1),
        jnp.flip(bwd_log, 1),
        True,
    )
    return (forward_out, forward_end, jnp.flip(backward_out, 1), backward_end)


def finish(query_rows, fwd_log, bwd_log, forward_out, backward_out, forward_entry, backward_entry):
    rising_decay = jnp.exp(jnp.cumsum(fwd_log, axis=1))
    falling_decay = jnp.exp(jnp.flip(jnp.cumsum(jnp.flip(bwd_log, 1), axis=1), 1))
    mixed = forward_out + backward_out
    mixed = mixed + jnp.einsum("xfj,xji->xfi", query_rows * rising_decay, forward_entry)
    mixed = mixed + jnp.einsum("xfj,xji->xfi", query_rows * falling_decay, backward_entry)
    return mixed * lax.rsqrt(jnp.mean(mixed * mixed, axis=-1, keepdims=True) + EPSILON)


def combine(earlier, later):
    return (earlier[0] * later[0], later[0][:, :, None] * earlier[1] + later[1])


def carry(decays, terms, backward):
    identity = (jnp.ones_like(decays), jnp.zeros_like(terms))
    return carried_in((decays, terms), SP, combine, identity, backward)[1]


def on_device(
    layer_grad,
    routes,
    route_weight,
    slot_tokens,
    gate_proj,
    up_proj,
    down_proj,
    out_proj,
    queries,
    keys,
    values,
    fwd_decay,
    bwd_decay,
):
    devices = lax.axis_size(SP)
    rows_here = layer_grad.shape[0]
    width = layer_grad.shape[1]
    slots = slot_tokens.shape[1]
    capacity = slots // devices
    expert_ids = routes.reshape(-1)
    ranks = slot_ranks(expert_ids, devices)
    kept = ranks < capacity
    target = jnp.where(kept, expert_ids * capacity + ranks, slots)
    sender = (
        jnp.full((slots + 1,), -1, jnp.int32)
        .at[target]
        .set(jnp.arange(2 * rows_here, dtype=jnp.int32))[:slots]
    )
    anchor = jnp.maximum(sender, 0)
    scaled = route_weight.reshape(-1)[anchor] * (sender >= 0).astype(jnp.float32)
    column_share = width // lax.axis_size("tp")
    own_slice = lax.dynamic_slice_in_dim(
        layer_grad, lax.axis_index("tp") * column_share, column_share, 1
    )
    outgoing = (own_slice[anchor // 2].astype(jnp.float32) * scaled[:, None]).astype(jnp.bfloat16)
    arrived = lax.all_to_all(
        outgoing.reshape(devices, capacity, column_share),
        SP,
        split_axis=0,
        concat_axis=0,
        tiled=True,
    ).reshape(slots, column_share)
    inbound = gathered_copies(arrived, "tp", 1)
    inputs = slot_tokens[0]
    w_gate = gate_proj[0]
    w_upper = up_proj[0]
    w_down = down_proj[0]
    gate = jnp.dot(inputs, w_gate, preferred_element_type=jnp.float32)
    upper = jnp.dot(inputs, w_upper, preferred_element_type=jnp.float32)
    sigma = jax.nn.sigmoid(gate)
    act = (gate * sigma * upper).astype(jnp.bfloat16)
    grad_down = lax.dot_general(
        act, inbound, (((0,), (0,)), ((), ())), preferred_element_type=jnp.float32
    )
    act_grad = lax.dot_general(
        inbound, w_down, (((1,), (1,)), ((), ())), preferred_element_type=jnp.float32
    )
    up_delta = (act_grad * gate * sigma).astype(jnp.bfloat16)
    gate_delta = (act_grad * upper * sigma * (1.0 + gate * (1.0 - sigma))).astype(jnp.bfloat16)
    grad_gate = lax.dot_general(
        inputs, gate_delta, (((0,), (0,)), ((), ())), preferred_element_type=jnp.float32
    )
    grad_up = lax.dot_general(
        inputs, up_delta, (((0,), (0,)), ((), ())), preferred_element_type=jnp.float32
    )
    slot_part = lax.dot_general(
        gate_delta, w_gate, (((1,), (1,)), ((), ())), preferred_element_type=jnp.float32
    )
    slot_part = slot_part + lax.dot_general(
        up_delta, w_upper, (((1,), (1,)), ((), ())), preferred_element_type=jnp.float32
    )
    safe_target = jnp.minimum(target, slots - 1)
    kept_float = kept.astype(jnp.float32)[:, None]
    quarter = width // lax.axis_size("tp")
    summed = lax.psum_scatter(slot_part.astype(jnp.bfloat16), "tp", scatter_dimension=1, tiled=True)
    backrows = lax.all_to_all(
        summed.reshape(devices, capacity, quarter), SP, split_axis=0, concat_axis=0, tiled=True
    ).reshape(slots, quarter)
    picked = backrows[safe_target].astype(jnp.float32) * kept_float
    moe_grad = jnp.sum(picked.reshape(rows_here, 2, quarter), axis=1)
    own_columns = lax.dynamic_slice_in_dim(layer_grad, lax.axis_index("tp") * quarter, quarter, 1)
    stream_part = (own_columns.astype(jnp.float32) + moe_grad).astype(jnp.bfloat16)
    stream_grad = lax.all_gather(stream_part, "tp", axis=1, tiled=True)
    scale = KEY_CHANNELS ** (-0.5)

    def split_heads(array, size):
        return array.astype(jnp.float32).reshape(rows_here, -1, size).transpose(1, 0, 2)

    def merge_heads(array):
        return array.transpose(1, 0, 2).reshape(rows_here, -1)

    query_heads = split_heads(queries, KEY_CHANNELS) * scale
    fwd_heads = split_heads(fwd_decay, KEY_CHANNELS)
    bwd_heads = split_heads(bwd_decay, KEY_CHANNELS)
    local_out, local_pull = jax.vjp(
        local_pass,
        query_heads,
        split_heads(keys, KEY_CHANNELS),
        split_heads(values, DV),
        fwd_heads,
        bwd_heads,
    )
    forward_out, forward_end, backward_out, backward_end = local_out
    fwd_total = jnp.exp(jnp.sum(fwd_heads, axis=1))
    bwd_total = jnp.exp(jnp.sum(bwd_heads, axis=1))
    forward_entry = carry(fwd_total, forward_end, False)
    backward_entry = carry(bwd_total, backward_end, True)
    mixed, finish_pull = jax.vjp(
        finish,
        query_heads,
        fwd_heads,
        bwd_heads,
        forward_out,
        backward_out,
        forward_entry,
        backward_entry,
    )
    mixed_rows = merge_heads(mixed).astype(jnp.bfloat16)
    proj_grad = sum_at_owner(
        lax.dot_general(
            stream_grad, mixed_rows, (((0,), (0,)), ((), ())), preferred_element_type=jnp.float32
        ),
        SP,
        0,
    )
    mixed_grad = jnp.dot(stream_grad, out_proj, preferred_element_type=jnp.float32)
    query_first, fwd_first, bwd_first, forward_cot, backward_cot, fwd_direct, bwd_direct = (
        finish_pull(split_heads(mixed_grad, DV))
    )
    fwd_after = carry(fwd_total, fwd_direct, True)
    bwd_after = carry(bwd_total, bwd_direct, False)
    query_second, key_part, value_part, fwd_unused, bwd_unused = local_pull(
        (forward_cot, fwd_after, backward_cot, bwd_after)
    )
    query_grad = (merge_heads(query_first + query_second) * scale).astype(jnp.bfloat16)
    return (
        grad_gate.astype(jnp.bfloat16)[None],
        grad_up.astype(jnp.bfloat16)[None],
        grad_down.astype(jnp.bfloat16)[None],
        proj_grad,
        query_grad,
        merge_heads(key_part).astype(jnp.bfloat16),
        merge_heads(value_part).astype(jnp.bfloat16),
    )


def solution(mesh):
    torus = Mesh(mesh.devices.reshape(8, 4, 2, mesh.shape["tp"]), ("sp_0", "sp_1", "sp_2", "tp"))
    in_specs = (
        P(SP, None),
        P(SP, None),
        P(SP, None),
        P(SP, None, None),
        P(SP, None, "tp"),
        P(SP, None, "tp"),
        P(SP, "tp", None),
        P(None, "tp"),
        P(SP, "tp"),
        P(SP, "tp"),
        P(SP, "tp"),
        P(SP, "tp"),
        P(SP, "tp"),
    )
    out_specs = (
        P(SP, None, "tp"),
        P(SP, None, "tp"),
        P(SP, "tp", None),
        P(SP, "tp"),
        P(SP, "tp"),
        P(SP, "tp"),
        P(SP, "tp"),
    )
    return jax.shard_map(
        on_device, mesh=torus, in_specs=in_specs, out_specs=out_specs, check_vma=False
    )
```

profile of v0, /device:TPU:1, one launch (start us, length us, event | category | flops | bytes accessed | tf_op | source)
XLA Modules:
  0.0 496.6 jit_solution(14228876233473937465)
XLA Ops:
  19.8 4.0 gather_fusion.1
  26.7 13.5 %all-to-all-start = ((bf16[64,9,512]{2,1,0:T(8,128)(2,1)}), bf16[64,9,512]{2,1,0:T(8,128)(2,1)}, u32[]{:S(2)}, u32[]{:S(2)}) async-start(bf16[64,9,512]{2,1,0:T(8,128)(2,1)} %multiply_convert_fusion), calls=%async_computation | async-start | bytes 2097152 | tf_op jit(solution)/shard_map/all_to_all | solution.py:213
  57.9 17.1 %while.115 = (s32[]{:T(128)}, f32[2,64,128]{2,1,0:T(8,128)S(1)}, f32[3,2,64,128]{3,2,1,0:T(8,128)}, f32[3,2,64,64]{3,2,1,0:T(8,128)}, f32[3,2,64,64]{3,2,1,0:T(8...) while((s32[]{:T(128)}, f32[2,64,128]{2,1,0:T(8,128)S(1)}, ...), condition=%wide.region_11.12_spmd.clone, body=%wide.region_9.11_spmd.clone.sunk | while | flops 8093699 | bytes 2081263 | solution.py:133
  82.1 12.8 %while.114 = (s32[]{:T(128)}, f32[2,64,128]{2,1,0:T(8,128)S(1)}, f32[3,2,64,128]{3,2,1,0:T(8,128)}, f32[3,2,64,64]{3,2,1,0:T(8,128)}, f32[3,2,64,64]{3,2,1,0:T(8...) while((s32[]{:T(128)}, f32[2,64,128]{2,1,0:T(8,128)S(1)}, ...), condition=%wide.region_8.9_spmd.clone, body=%wide.region_6.8_spmd.clone.sunk | while | flops 8093699 | bytes 1981671 | solution.py:133
  103.1 10.3 %all-gather.13 = f32[4,129,128]{2,1,0:T(8,128)S(1)} all-gather(f32[1,129,128]{2,1,0:T(8,128)S(1)} %maximum_bitcast_fusion), channel_id=3, replica_groups=mesh['sp_0'=8,'sp_1'=4,'sp_2'=2,'tp'=4] {'sp_1'}, dimensions={0}, use_global_device_ids=true | all-gather | bytes 330240 | tf_op jit(solution)/shard_map/all_gather | solution.py:28
  118.3 4.6 all-to-all-start.1
  123.0 4.2 all-gather.15
  127.9 10.8 %all-gather.16 = f32[4,129,128]{2,1,0:T(8,128)S(1)} all-gather(f32[1,129,128]{2,1,0:T(8,128)S(1)} %maximum_bitcast_fusion.2), channel_id=6, replica_groups=mesh['sp_0'=8,'sp_1'=4,'sp_2'=2,'tp'=4] {'sp_1'}, dimensions={0}, use_global_device_ids=true | all-gather | bytes 330240 | tf_op jit(solution)/shard_map/all_gather | solution.py:28
  144.0 5.6 %all-to-all-done.1 = bf16[4,576,512]{2,1,0:T(8,128)(2,1)} async-done(((bf16[4,576,512]{2,1,0:T(8,128)(2,1)}), bf16[4,576,512]{2,1,0:T(8,128)(2,1)}, u32[]{:S(2)}, u32[]{:S(2)}) %all-to-all-start.1) | async-done | bytes 2359328 | tf_op jit(solution)/shard_map/all_to_all | solution.py:70
  157.4 21.8 %all-gather.14 = f32[8,129,128]{2,1,0:T(8,128)S(1)} all-gather(f32[1,129,128]{2,1,0:T(8,128)S(1)} %maximum_bitcast_fusion.1), channel_id=4, replica_groups=mesh['sp_0'=8,'sp_1'=4,'sp_2'=2,'tp'=4] {'sp_0'}, dimensions={0}, use_global_device_ids=true | all-gather | bytes 594432 | tf_op jit(solution)/shard_map/all_gather | solution.py:28
  179.2 20.9 %all-gather.17 = f32[8,129,128]{2,1,0:T(8,128)S(1)} all-gather(f32[1,129,128]{2,1,0:T(8,128)S(1)} %maximum_bitcast_fusion.3), channel_id=7, replica_groups=mesh['sp_0'=8,'sp_1'=4,'sp_2'=2,'tp'=4] {'sp_0'}, dimensions={0}, use_global_device_ids=true | all-gather | bytes 594432 | tf_op jit(solution)/shard_map/all_gather | solution.py:28
  234.4 20.6 %all-to-all-start.2 = ((bf16[64,9,512]{2,1,0:T(8,128)(2,1)}), bf16[64,9,512]{2,1,0:T(8,128)(2,1)}, u32[]{:S(2)}, u32[]{:S(2)}) async-start(bf16[64,9,512]{2,1,0:T(8,128)(2,1)} %reshape.1346), calls=%async_computation.3 | async-start | bytes 2097152 | tf_op jit(solution)/shard_map/all_to_all | solution.py:253
  265.0 4.0 fusion.172
  269.0 14.0 %all-to-all-done.2 = bf16[64,9,512]{2,1,0:T(8,128)(2,1)} async-done(((bf16[64,9,512]{2,1,0:T(8,128)(2,1)}), bf16[64,9,512]{2,1,0:T(8,128)(2,1)}, u32[]{:S(2)}, u32[]{:S(2)}) %all-to-all-start.2) | async-done | bytes 589856 | tf_op jit(solution)/shard_map/all_to_all | solution.py:253
  291.6 11.2 %all_gather.75 = bf16[192,2048]{1,0:T(8,128)(2,1)S(1)} all-gather(bf16[192,512]{1,0:T(8,128)(2,1)S(1)} %add_convert_fusion.1), channel_id=1, replica_groups=mesh['sp_0'=8,'sp_1'=4,'sp_2'=2,'tp'=4] {'tp'}, dimensions={1}, use_global_device_ids=true | all-gather | bytes 983040 | tf_op jit(solution)/shard_map/all_gather | solution.py:260
  305.0 5.7 %all-gather.21 = f32[2,129,128]{2,1,0:T(8,128)S(1)} all-gather(f32[1,129,128]{2,1,0:T(8,128)S(1)} %fusion.205), channel_id=11, replica_groups=mesh['sp_0'=8,'sp_1'=4,'sp_2'=2,'tp'=4] {'sp_2'}, dimensions={0}, use_global_device_ids=true | all-gather | bytes 198144 | tf_op jit(solution)/shard_map/all_gather | solution.py:28
  312.1 10.1 %all-gather.22 = f32[4,129,128]{2,1,0:T(8,128)S(1)} all-gather(f32[1,129,128]{2,1,0:T(8,128)S(1)} %maximum_bitcast_fusion.6), channel_id=12, replica_groups=mesh['sp_0'=8,'sp_1'=4,'sp_2'=2,'tp'=4] {'sp_1'}, dimensions={0}, use_global_device_ids=true | all-gather | bytes 330240 | tf_op jit(solution)/shard_map/all_gather | solution.py:28
  323.6 19.7 %all-gather.23 = f32[8,129,128]{2,1,0:T(8,128)S(1)} all-gather(f32[1,129,128]{2,1,0:T(8,128)S(1)} %maximum_bitcast_fusion.7), channel_id=13, replica_groups=mesh['sp_0'=8,'sp_1'=4,'sp_2'=2,'tp'=4] {'sp_0'}, dimensions={0}, use_global_device_ids=true | all-gather | bytes 594432 | tf_op jit(solution)/shard_map/all_gather | solution.py:28
  345.0 10.6 %all-gather.18 = f32[2,129,128]{2,1,0:T(8,128)S(1)} all-gather(f32[1,129,128]{2,1,0:T(8,128)S(1)} %fusion.203), channel_id=8, replica_groups=mesh['sp_0'=8,'sp_1'=4,'sp_2'=2,'tp'=4] {'sp_2'}, dimensions={0}, use_global_device_ids=true | all-gather | bytes 198144 | tf_op jit(solution)/shard_map/all_gather | solution.py:28
  356.9 10.0 %all-gather.19 = f32[4,129,128]{2,1,0:T(8,128)S(1)} all-gather(f32[1,129,128]{2,1,0:T(8,128)S(1)} %maximum_bitcast_fusion.4), channel_id=9, replica_groups=mesh['sp_0'=8,'sp_1'=4,'sp_2'=2,'tp'=4] {'sp_1'}, dimensions={0}, use_global_device_ids=true | all-gather | bytes 330240 | tf_op jit(solution)/shard_map/all_gather | solution.py:28
  368.4 20.1 %all-gather.20 = f32[8,129,128]{2,1,0:T(8,128)S(1)} all-gather(f32[1,129,128]{2,1,0:T(8,128)S(1)} %maximum_bitcast_fusion.5), channel_id=10, replica_groups=mesh['sp_0'=8,'sp_1'=4,'sp_2'=2,'tp'=4] {'sp_0'}, dimensions={0}, use_global_device_ids=true | all-gather | bytes 594432 | tf_op jit(solution)/shard_map/all_gather | solution.py:28
  396.1 13.9 %all-to-all-start.3 = ((f32[64,32,256]{2,1,0:T(8,128)}), f32[64,32,256]{2,1,0:T(8,128)}, u32[]{:S(2)}, u32[]{:S(2)}) async-start(f32[64,32,256]{2,1,0:T(8,128)} %fusion.253), calls=%async_computation.4 | async-start | bytes 4194304 | tf_op jit(solution)/shard_map/all_to_all | solution.py:93
  422.0 23.2 %while.112 = (s32[]{:T(128)}, f32[2,64,128]{2,1,0:T(8,128)S(1)}, f32[3,2,64,64]{3,2,1,0:T(8,128)S(1)}, f32[3,2,64,64]{3,2,1,0:T(8,128)S(1)}, f32[3,2,64,128]{3,2...) while((s32[]{:T(128)}, f32[2,64,128]{2,1,0:T(8,128)S(1)}, ...), condition=%wide.region_22.23_spmd.clone, body=%wide.region_21.22_spmd.clone.sunk | while | flops 14802947 | bytes 1518041 | solution.py:133
  449.0 24.9 %while.113 = (s32[]{:T(128)}, f32[2,64,128]{2,1,0:T(8,128)S(1)}, f32[3,2,64,64]{3,2,1,0:T(8,128)S(1)}, f32[3,2,64,64]{3,2,1,0:T(8,128)}, f32[3,2,64,128]{3,2,0,1...) while((s32[]{:T(128)}, f32[2,64,128]{2,1,0:T(8,128)S(1)}, ...), condition=%wide.region_24.25_spmd.clone, body=%wide.region_23.24_spmd.clone.sunk | while | flops 14802947 | bytes 1501393 | solution.py:133
  (648 shorter events, 244.7 us)
Async XLA Ops:
  7.2 132.2 %copy-start = (bf16[1,576,2048]{2,1,0:T(8,128)(2,1)S(1)}, bf16[1,576,2048]{2,1,0:T(8,128)(2,1)}, u32[]{:S(2)}) copy-start(bf16[1,576,2048]{2,1,0:T(8,128)(2,1)} %param.24) | copy-start | bytes 7077892
  26.7 88.6 %all-to-all-start = ((bf16[64,9,512]{2,1,0:T(8,128)(2,1)}), bf16[64,9,512]{2,1,0:T(8,128)(2,1)}, u32[]{:S(2)}, u32[]{:S(2)}) async-start(bf16[64,9,512]{2,1,0:T(8,128)(2,1)} %multiply_convert_fusion), calls=%async_computation | async-start | bytes 2097152 | tf_op jit(solution)/shard_map/all_to_all | solution.py:213
  114.1 109.7 %copy-start.62 = (f32[2,64]{1,0:T(2,128)}, f32[2,64]{1,0:T(2,128)S(1)}, u32[]{:S(2)}) copy-start(f32[2,64]{1,0:T(2,128)S(1)} %squeeze.560) | copy-start | bytes 1540
  114.2 109.7 %copy-start.64 = (f32[2,64]{1,0:T(2,128)}, f32[2,64]{1,0:T(2,128)S(1)}, u32[]{:S(2)}) copy-start(f32[2,64]{1,0:T(2,128)S(1)} %squeeze.559) | copy-start | bytes 1540
  114.3 109.6 %copy-start.66 = (f32[2,64]{1,0:T(2,128)}, f32[2,64]{1,0:T(2,128)S(1)}, u32[]{:S(2)}) copy-start(f32[2,64]{1,0:T(2,128)S(1)} %squeeze.558) | copy-start | bytes 1540
  115.0 108.9 %copy-start.68 = (f32[2,64]{1,0:T(2,128)}, f32[2,64]{1,0:T(2,128)S(1)}, u32[]{:S(2)}) copy-start(f32[2,64]{1,0:T(2,128)S(1)} %squeeze.562) | copy-start | bytes 1540
  118.3 31.3 %all-to-all-start.1 = ((bf16[4,576,512]{2,1,0:T(8,128)(2,1)}), bf16[4,576,512]{2,1,0:T(8,128)(2,1)}, u32[]{:S(2)}, u32[]{:S(2)}) async-start(bf16[4,576,512]{2,1,0:T(8,128)(2,1)} %broadcast_in_dim.154), calls=%async_computation.1 | async-start | bytes 4718592 | tf_op jit(solution)/shard_map/all_to_all | solution.py:70
  122.9 109.2 %reduce-scatter.2.cloned.1.call-start = ((), (), s32[]{:S(2)}) async-start(), calls=%async_computation.5 | async-start | bytes 2949120 | tf_op jit(solution)/shard_map/reduce_scatter | solution.py:252
  157.2 46.5 %copy-start.16 = (f32[192,128]{0,1:T(8,128)S(1)}, f32[192,128]{0,1:T(8,128)}, u32[]{:S(2)}) copy-start(f32[192,128]{0,1:T(8,128)} %copy-done.15) | copy-start | bytes 294916
  157.2 51.9 %copy-start.116 = (f32[128]{0:T(128)S(1)}, f32[128]{0:T(128)}, u32[]{:S(2)}) copy-start(f32[128]{0:T(128)} %get-tuple-element.1529) | copy-start | bytes 1540
  157.2 66.6 %copy-start.61 = (s32[384]{0:T(512)S(1)}, s32[384]{0:T(512)}, u32[]{:S(2)}) copy-start(s32[384]{0:T(512)} %get-tuple-element.1545) | copy-start | bytes 4612
  157.2 66.7 %copy-start.91 = (f32[2,64]{1,0:T(2,128)S(1)}, f32[2,64]{1,0:T(2,128)}, u32[]{:S(2)}) copy-start(f32[2,64]{1,0:T(2,128)} %squeeze.557) | copy-start | bytes 1540
  157.2 66.7 %copy-start.92 = (f32[2,64]{1,0:T(2,128)S(1)}, f32[2,64]{1,0:T(2,128)}, u32[]{:S(2)}) copy-start(f32[2,64]{1,0:T(2,128)} %squeeze.561) | copy-start | bytes 1540
  234.4 48.6 %all-to-all-start.2 = ((bf16[64,9,512]{2,1,0:T(8,128)(2,1)}), bf16[64,9,512]{2,1,0:T(8,128)(2,1)}, u32[]{:S(2)}, u32[]{:S(2)}) async-start(bf16[64,9,512]{2,1,0:T(8,128)(2,1)} %reshape.1346), calls=%async_computation.3 | async-start | bytes 2097152 | tf_op jit(solution)/shard_map/all_to_all | solution.py:253
  256.5 46.7 %copy-start.45 = (bf16[2,64,128]{2,1,0:T(8,128)(2,1)}, bf16[2,64,128]{2,1,0:T(8,128)(2,1)S(1)}, u32[]{:S(2)}) copy-start(bf16[2,64,128]{2,1,0:T(8,128)(2,1)S(1)} %add_add_fusion.3) | copy-start | bytes 98308
  304.8 40.2 %copy-start.4 = (bf16[2,192,128]{2,1,0:T(8,128)(2,1)}, bf16[2,192,128]{2,1,0:T(8,128)(2,1)S(1)}, u32[]{:S(2)}) copy-start(bf16[2,192,128]{2,1,0:T(8,128)(2,1)S(1)} %add_add_fusion) | copy-start | bytes 294916
  304.8 40.2 %copy-start.83 = (f32[1,128]{1,0:T(1,128)S(1)}, f32[1,128]{1,0:T(1,128)}, u32[]{:S(2)}) copy-start(f32[1,128]{1,0:T(1,128)} %copy-done.82) | copy-start | bytes 1540
  345.0 44.9 %copy-start.5 = (bf16[2,192,128]{2,1,0:T(8,128)(2,1)S(1)}, bf16[2,192,128]{2,1,0:T(8,128)(2,1)}, u32[]{:S(2)}) copy-start(bf16[2,192,128]{2,1,0:T(8,128)(2,1)} %copy-done.4) | copy-start | bytes 294916
  366.9 25.7 %copy-start.44 = (bf16[192,2,128]{2,0,1:T(8,128)(2,1)S(1)}, bf16[192,2,128]{2,0,1:T(8,128)(2,1)}, u32[]{:S(2)}) copy-start(bf16[192,2,128]{2,0,1:T(8,128)(2,1)} %fusion.197) | copy-start | bytes 294916
  396.1 91.3 %all-to-all-start.3 = ((f32[64,32,256]{2,1,0:T(8,128)}), f32[64,32,256]{2,1,0:T(8,128)}, u32[]{:S(2)}, u32[]{:S(2)}) async-start(f32[64,32,256]{2,1,0:T(8,128)} %fusion.253), calls=%async_computation.4 | async-start | bytes 4194304 | tf_op jit(solution)/shard_map/all_to_all | solution.py:93
  422.0 27.0 %copy-start.3 = (bf16[3,2,64,128]{3,2,1,0:T(8,128)(2,1)S(1)}, bf16[3,2,64,128]{3,2,1,0:T(8,128)(2,1)}, u32[]{:S(2)}) copy-start(bf16[3,2,64,128]{3,2,1,0:T(8,128)(2,1)} %copy-done.2) | copy-start | bytes 294916
  448.9 33.0 %copy-start.14 = (f32[2,256,64]{1,2,0:T(8,128)S(1)}, f32[2,256,64]{1,2,0:T(8,128)}, u32[]{:S(2)}) copy-start(f32[2,256,64]{1,2,0:T(8,128)} %reverse.7) | copy-start | bytes 393220
  449.0 33.0 %copy-start.46 = (bf16[2,64,128]{2,1,0:T(8,128)(2,1)S(1)}, bf16[2,64,128]{2,1,0:T(8,128)(2,1)}, u32[]{:S(2)}) copy-start(bf16[2,64,128]{2,1,0:T(8,128)(2,1)} %copy-done.45) | copy-start | bytes 98308
  449.0 33.2 %copy-start.19 = (f32[2,256,64]{1,2,0:T(8,128)S(1)}, f32[2,256,64]{1,2,0:T(8,128)}, u32[]{:S(2)}) copy-start(f32[2,256,64]{1,2,0:T(8,128)} %copy-done.17) | copy-start | bytes 393220
  (103 other events, 1502.4 us)
Sparse Core Ops, SparseCore 0:
  157.3 35.1 reduce-scatter.1
where the time goes:
time: 502 us; the launch traced here: 497 us
  blocking collectives  157 us (31%)
  local copies, waits for them, and re-layouts  119 us (24%)
  matrix products  84.1 us (17%)
  starting transfers between devices  52.6 us (10%)
  other arithmetic  47.3 us (9%)
  waiting for transfers between devices  19.6 us (4%)
  between operations  16 us (3%)
    all_gather x12, blocking collectives, all_in_one(): both, at, found = (lax.all_gather(jnp.concatenate(lines), axis), 0, {})  146 us
    unnamed x272, local copies, waits for them, and re-layouts  24 us
    dot_general x18, matrix products, advance(): jnp.einsum('hik,hjk->hij', query_block * jnp.exp(running_total - middle),...  21 us
    all_to_all x1, starting transfers between devices, on_device(): lax.all_to_all(summed.reshape(devices, capacity, quarter), SP, split_axis...  20.6 us
    dot_general x18, matrix products, advance(): jnp.einsum('zuw,zwo->zuo', query_block * jnp.exp(running_total), carried_...  16.4 us
    mul x32, local copies, waits for them, and re-layouts, combine(): return (earlier[0] * later[0], later[0][:, :, None] * earlier[1] + later[1])  15.3 us
    all_to_all x1, waiting for transfers between devices, on_device(): lax.all_to_all(summed.reshape(devices, capacity, quarter), SP, split_axis...  14 us
    all_to_all x1, starting transfers between devices, sum_at_owner(): lax.all_to_all(pieces, axis, split_axis=0, concat_axis=0, tiled=True)  13.9 us
  transfers between devices with their start and end apart: 5, of which 2 were waited for; matrix products, arithmetic and copies ran while one was open for 38% of the time, Pallas kernels for 0%

commit v1 on v0

--- a/solution.py
+++ b/solution.py
@@ -257,7 +257,9 @@
     moe_grad = jnp.sum(picked.reshape(rows_here, 2, quarter), axis=1)
     own_columns = lax.dynamic_slice_in_dim(layer_grad, lax.axis_index("tp") * quarter, quarter, 1)
     stream_part = (own_columns.astype(jnp.float32) + moe_grad).astype(jnp.bfloat16)
-    stream_grad = lax.all_gather(stream_part, "tp", axis=1, tiled=True)
+    stream_grad = jnp.concatenate(
+        lax.all_to_all(jnp.stack([stream_part] * lax.axis_size("tp")), "tp", 0, 0), axis=1
+    )
     scale = KEY_CHANNELS ** (-0.5)
 
     def split_heads(array, size):

time: 502 us -> 538 us (1.072)
  local copies, waits for them, and re-layouts: 119 us -> 152 us
  other arithmetic: 47.3 us -> 62.1 us
  blocking collectives: 157 us -> 143 us
  starting transfers between devices: 52.6 us -> 60.8 us
  waiting for transfers between devices: 19.6 us -> 11.5 us
    all_to_all x1, waiting for transfers between devices: 14 us -> 0.01 us  [on_device(): lax.all_to_all(summed.reshape(devices, capacity, quarter), SP, split_axis...]
    mul x32, local copies, waits for them, and re-layouts: 15.3 us -> 26.9 us  [combine(): return (earlier[0] * later[0], later[0][:, :, None] * earlier[1] + later[1])]
    all_gather x1 -> x0, blocking collectives: 11.2 us -> none  [on_device(): stream_grad = lax.all_gather(stream_part, 'tp', axis=1, tiled=True)]
    squeeze x24, local copies, waits for them, and re-layouts: 6.05 us -> 15.9 us  [carried_in(): total = combine(total, jax.tree.map(lambda part: part[k], pieces))]
    another operation x25 -> x26, local copies, waits for them, and re-layouts: 12.7 us -> 15.7 us
    unnamed x272 -> x218, local copies, waits for them, and re-layouts: 24 us -> 21.8 us
  transfers between devices with their start and end apart: 5 -> 6, of which waited for: 2 -> 2; matrix products, arithmetic and copies ran while one was open for 38% -> 43% of each run, Pallas kernels for 0% -> 0%
where the time goes in v1:
time: 538 us; the launch traced here: 533 us
  local copies, waits for them, and re-layouts  152 us (28%)
  blocking collectives  143 us (27%)
  matrix products  87.6 us (16%)
  other arithmetic  62.1 us (12%)
  starting transfers between devices  60.8 us (11%)
  between operations  15.4 us (3%)
  waiting for transfers between devices  11.5 us (2%)
    all_gather x12, blocking collectives, all_in_one(): both, at, found = (lax.all_gather(jnp.concatenate(lines), axis), 0, {})  143 us
    mul x32, local copies, waits for them, and re-layouts, combine(): return (earlier[0] * later[0], later[0][:, :, None] * earlier[1] + later[1])  26.9 us
    all_to_all x1, starting transfers between devices, on_device(): lax.all_to_all(summed.reshape(devices, capacity, quarter), SP, split_axis...  22.1 us
    unnamed x218, local copies, waits for them, and re-layouts  21.8 us
    dot_general x18, matrix products, advance(): jnp.einsum('hik,hjk->hij', query_block * jnp.exp(running_total - middle),...  21 us
    all_to_all x1, starting transfers between devices, sum_at_owner(): lax.all_to_all(pieces, axis, split_axis=0, concat_axis=0, tiled=True)  17 us
    dot_general x18, matrix products, advance(): jnp.einsum('zuw,zwo->zuo', query_block * jnp.exp(running_total), carried_...  16.4 us
    squeeze x24, local copies, waits for them, and re-layouts, carried_in(): total = combine(total, jax.tree.map(lambda part: part[k], pieces))  15.9 us
  transfers between devices with their start and end apart: 6, of which 2 were waited for; matrix products, arithmetic and copies ran while one was open for 43% of the time, Pallas kernels for 0%

profile of v1, /device:TPU:1, one launch (start us, length us, event | category | flops | bytes accessed | tf_op | source)
XLA Modules:
  0.0 532.6 jit_solution(18075352572923379351)
XLA Ops:
  19.8 4.0 gather_fusion.1
  26.7 13.5 %all-to-all-start = ((bf16[64,9,512]{2,1,0:T(8,128)(2,1)}), bf16[64,9,512]{2,1,0:T(8,128)(2,1)}, u32[]{:S(2)}, u32[]{:S(2)}) async-start(bf16[64,9,512]{2,1,0:T(8,128)(2,1)} %multiply_convert_fusion), calls=%async_computation | async-start | bytes 2097152 | tf_op jit(solution)/shard_map/all_to_all | solution.py:213
  57.8 17.1 %while.115 = (s32[]{:T(128)}, f32[2,64,128]{2,1,0:T(8,128)S(1)}, f32[3,2,64,128]{3,2,1,0:T(8,128)}, f32[3,2,64,64]{3,2,1,0:T(8,128)}, f32[3,2,64,64]{3,2,1,0:T(8...) while((s32[]{:T(128)}, f32[2,64,128]{2,1,0:T(8,128)S(1)}, ...), condition=%wide.region_11.12_spmd.clone, body=%wide.region_9.11_spmd.clone.sunk | while | flops 8093699 | bytes 2081263 | solution.py:133
  82.1 12.8 %while.114 = (s32[]{:T(128)}, f32[2,64,128]{2,1,0:T(8,128)S(1)}, f32[3,2,64,128]{3,2,1,0:T(8,128)}, f32[3,2,64,64]{3,2,1,0:T(8,128)}, f32[3,2,64,64]{3,2,1,0:T(8...) while((s32[]{:T(128)}, f32[2,64,128]{2,1,0:T(8,128)S(1)}, ...), condition=%wide.region_8.9_spmd.clone, body=%wide.region_6.8_spmd.clone.sunk | while | flops 8093699 | bytes 1981671 | solution.py:133
  105.5 4.6 all-to-all-start.1
  112.8 11.1 %all-gather.13 = f32[4,129,128]{2,1,0:T(8,128)S(1)} all-gather(f32[1,129,128]{2,1,0:T(8,128)S(1)} %maximum_bitcast_fusion), channel_id=3, replica_groups=mesh['sp_0'=8,'sp_1'=4,'sp_2'=2,'tp'=4] {'sp_1'}, dimensions={0}, use_global_device_ids=true | all-gather | bytes 330240 | tf_op jit(solution)/shard_map/all_gather | solution.py:28
  130.0 9.1 %all-to-all-done.1 = bf16[4,576,512]{2,1,0:T(8,128)(2,1)} async-done(((bf16[4,576,512]{2,1,0:T(8,128)(2,1)}), bf16[4,576,512]{2,1,0:T(8,128)(2,1)}, u32[]{:S(2)}, u32[]{:S(2)}) %all-to-all-start.1) | async-done | bytes 2359328 | tf_op jit(solution)/shard_map/all_to_all | solution.py:70
  159.7 11.2 %all-gather.16 = f32[4,129,128]{2,1,0:T(8,128)S(1)} all-gather(f32[1,129,128]{2,1,0:T(8,128)S(1)} %maximum_bitcast_fusion.2), channel_id=6, replica_groups=mesh['sp_0'=8,'sp_1'=4,'sp_2'=2,'tp'=4] {'sp_1'}, dimensions={0}, use_global_device_ids=true | all-gather | bytes 330240 | tf_op jit(solution)/shard_map/all_gather | solution.py:28
  181.5 3.3 reduce-window.26
  201.0 21.1 %all-gather.14 = f32[8,129,128]{2,1,0:T(8,128)S(1)} all-gather(f32[1,129,128]{2,1,0:T(8,128)S(1)} %maximum_bitcast_fusion.1), channel_id=4, replica_groups=mesh['sp_0'=8,'sp_1'=4,'sp_2'=2,'tp'=4] {'sp_0'}, dimensions={0}, use_global_device_ids=true | all-gather | bytes 594432 | tf_op jit(solution)/shard_map/all_gather | solution.py:28
  222.1 20.2 %all-gather.17 = f32[8,129,128]{2,1,0:T(8,128)S(1)} all-gather(f32[1,129,128]{2,1,0:T(8,128)S(1)} %maximum_bitcast_fusion.3), channel_id=7, replica_groups=mesh['sp_0'=8,'sp_1'=4,'sp_2'=2,'tp'=4] {'sp_0'}, dimensions={0}, use_global_device_ids=true | all-gather | bytes 594432 | tf_op jit(solution)/shard_map/all_gather | solution.py:28
  247.6 22.1 %all-to-all-start.2 = ((bf16[64,9,512]{2,1,0:T(8,128)(2,1)}), bf16[64,9,512]{2,1,0:T(8,128)(2,1)}, u32[]{:S(2)}, u32[]{:S(2)}) async-start(bf16[64,9,512]{2,1,0:T(8,128)(2,1)} %reshape.1353), calls=%async_computation.3 | async-start | bytes 2097152 | tf_op jit(solution)/shard_map/all_to_all | solution.py:253
  313.0 3.5 all-to-all-start.3
  321.7 4.0 fusion.172
  337.1 3.2 all-gather.21
  341.6 10.5 %all-gather.22 = f32[4,129,128]{2,1,0:T(8,128)S(1)} all-gather(f32[1,129,128]{2,1,0:T(8,128)S(1)} %maximum_bitcast_fusion.6), channel_id=12, replica_groups=mesh['sp_0'=8,'sp_1'=4,'sp_2'=2,'tp'=4] {'sp_1'}, dimensions={0}, use_global_device_ids=true | all-gather | bytes 330240 | tf_op jit(solution)/shard_map/all_gather | solution.py:28
  353.6 21.1 %all-gather.23 = f32[8,129,128]{2,1,0:T(8,128)S(1)} all-gather(f32[1,129,128]{2,1,0:T(8,128)S(1)} %maximum_bitcast_fusion.7), channel_id=13, replica_groups=mesh['sp_0'=8,'sp_1'=4,'sp_2'=2,'tp'=4] {'sp_0'}, dimensions={0}, use_global_device_ids=true | all-gather | bytes 594432 | tf_op jit(solution)/shard_map/all_gather | solution.py:28
  376.4 9.8 %all-gather.18 = f32[2,129,128]{2,1,0:T(8,128)S(1)} all-gather(f32[1,129,128]{2,1,0:T(8,128)S(1)} %fusion.200), channel_id=8, replica_groups=mesh['sp_0'=8,'sp_1'=4,'sp_2'=2,'tp'=4] {'sp_2'}, dimensions={0}, use_global_device_ids=true | all-gather | bytes 198144 | tf_op jit(solution)/shard_map/all_gather | solution.py:28
  387.6 10.0 %all-gather.19 = f32[4,129,128]{2,1,0:T(8,128)S(1)} all-gather(f32[1,129,128]{2,1,0:T(8,128)S(1)} %maximum_bitcast_fusion.4), channel_id=9, replica_groups=mesh['sp_0'=8,'sp_1'=4,'sp_2'=2,'tp'=4] {'sp_1'}, dimensions={0}, use_global_device_ids=true | all-gather | bytes 330240 | tf_op jit(solution)/shard_map/all_gather | solution.py:28
  399.0 20.4 %all-gather.20 = f32[8,129,128]{2,1,0:T(8,128)S(1)} all-gather(f32[1,129,128]{2,1,0:T(8,128)S(1)} %maximum_bitcast_fusion.5), channel_id=10, replica_groups=mesh['sp_0'=8,'sp_1'=4,'sp_2'=2,'tp'=4] {'sp_0'}, dimensions={0}, use_global_device_ids=true | all-gather | bytes 594432 | tf_op jit(solution)/shard_map/all_gather | solution.py:28
  425.6 3.0 fusion.250
  428.9 17.0 %all-to-all-start.4 = ((f32[64,32,256]{2,1,0:T(8,128)}), f32[64,32,256]{2,1,0:T(8,128)}, u32[]{:S(2)}, u32[]{:S(2)}) async-start(f32[64,32,256]{2,1,0:T(8,128)} %fusion.250), calls=%async_computation.5 | async-start | bytes 4194304 | tf_op jit(solution)/shard_map/all_to_all | solution.py:93
  458.1 23.2 %while.112 = (s32[]{:T(128)}, f32[2,64,128]{2,1,0:T(8,128)S(1)}, f32[3,2,64,64]{3,2,1,0:T(8,128)S(1)}, f32[3,2,64,64]{3,2,1,0:T(8,128)S(1)}, f32[3,2,64,128]{3,2...) while((s32[]{:T(128)}, f32[2,64,128]{2,1,0:T(8,128)S(1)}, ...), condition=%wide.region_22.23_spmd.clone, body=%wide.region_21.22_spmd.clone.sunk | while | flops 14802947 | bytes 1518041 | solution.py:133
  485.1 24.9 %while.113 = (s32[]{:T(128)}, f32[2,64,128]{2,1,0:T(8,128)S(1)}, f32[3,2,64,64]{3,2,1,0:T(8,128)S(1)}, f32[3,2,64,64]{3,2,1,0:T(8,128)}, f32[3,2,64,128]{3,2,0,1...) while((s32[]{:T(128)}, f32[2,64,128]{2,1,0:T(8,128)S(1)}, ...), condition=%wide.region_24.25_spmd.clone, body=%wide.region_23.24_spmd.clone.sunk | while | flops 14802947 | bytes 1501393 | solution.py:133
  (600 shorter events, 294.2 us)
Async XLA Ops:
  7.2 118.2 %copy-start = (bf16[1,576,2048]{2,1,0:T(8,128)(2,1)S(1)}, bf16[1,576,2048]{2,1,0:T(8,128)(2,1)}, u32[]{:S(2)}) copy-start(bf16[1,576,2048]{2,1,0:T(8,128)(2,1)} %param.24) | copy-start | bytes 7077892
  26.7 75.8 %all-to-all-start = ((bf16[64,9,512]{2,1,0:T(8,128)(2,1)}), bf16[64,9,512]{2,1,0:T(8,128)(2,1)}, u32[]{:S(2)}, u32[]{:S(2)}) async-start(bf16[64,9,512]{2,1,0:T(8,128)(2,1)} %multiply_convert_fusion), calls=%async_computation | async-start | bytes 2097152 | tf_op jit(solution)/shard_map/all_to_all | solution.py:213
  105.5 33.6 %all-to-all-start.1 = ((bf16[4,576,512]{2,1,0:T(8,128)(2,1)}), bf16[4,576,512]{2,1,0:T(8,128)(2,1)}, u32[]{:S(2)}, u32[]{:S(2)}) async-start(bf16[4,576,512]{2,1,0:T(8,128)(2,1)} %broadcast_in_dim.154), calls=%async_computation.1 | async-start | bytes 4718592 | tf_op jit(solution)/shard_map/all_to_all | solution.py:70
  110.1 135.3 %reduce-scatter.2.cloned.1.call-start = ((), (), s32[]{:S(2)}) async-start(), calls=%async_computation.6 | async-start | bytes 2949120 | tf_op jit(solution)/shard_map/reduce_scatter | solution.py:252
  199.3 46.0 %copy-start.30 = (f32[2,192,128]{2,1,0:T(8,128)S(1)}, f32[2,192,128]{2,1,0:T(8,128)}, u32[]{:S(2)}) copy-start(f32[2,192,128]{2,1,0:T(8,128)} %rev.39) | copy-start | bytes 589828
  199.3 46.0 %copy-start.31 = (f32[2,3,64,128]{3,2,1,0:T(8,128)S(1)}, f32[2,3,64,128]{3,2,1,0:T(8,128)}, u32[]{:S(2)}) copy-start(f32[2,3,64,128]{3,2,1,0:T(8,128)} %copy.184) | copy-start | bytes 589828
  247.6 46.1 %copy-start.34 = (f32[2,256,64]{1,2,0:T(8,128)S(1)}, f32[2,256,64]{1,2,0:T(8,128)}, u32[]{:S(2)}) copy-start(f32[2,256,64]{1,2,0:T(8,128)} %bitcast_bitcast_fusion) | copy-start | bytes 393220
  247.6 46.9 %copy-start.53 = (s32[384]{0:T(512)S(1)}, s32[384]{0:T(512)}, u32[]{:S(2)}) copy-start(s32[384]{0:T(512)} %get-tuple-element.1545) | copy-start | bytes 4612
  247.6 47.0 %copy-start.57 = (f32[2,64]{1,0:T(2,128)S(1)}, f32[2,64]{1,0:T(2,128)}, u32[]{:S(2)}) copy-start(f32[2,64]{1,0:T(2,128)} %squeeze.560) | copy-start | bytes 1540
  247.6 47.0 %copy-start.58 = (f32[2,64]{1,0:T(2,128)S(1)}, f32[2,64]{1,0:T(2,128)}, u32[]{:S(2)}) copy-start(f32[2,64]{1,0:T(2,128)} %squeeze.559) | copy-start | bytes 1540
  247.6 48.6 %copy-start.11 = (f32[2,256,64]{1,2,0:T(8,128)S(1)}, f32[2,256,64]{1,2,0:T(8,128)}, u32[]{:S(2)}) copy-start(f32[2,256,64]{1,2,0:T(8,128)} %bitcast_bitcast_fusion.1) | copy-start | bytes 393220
  247.6 56.0 %all-to-all-start.2 = ((bf16[64,9,512]{2,1,0:T(8,128)(2,1)}), bf16[64,9,512]{2,1,0:T(8,128)(2,1)}, u32[]{:S(2)}, u32[]{:S(2)}) async-start(bf16[64,9,512]{2,1,0:T(8,128)(2,1)} %reshape.1353), calls=%async_computation.3 | async-start | bytes 2097152 | tf_op jit(solution)/shard_map/all_to_all | solution.py:253
  269.7 27.4 %copy-start.54 = (f32[2,64]{1,0:T(2,128)S(1)}, f32[2,64]{1,0:T(2,128)}, u32[]{:S(2)}) copy-start(f32[2,64]{1,0:T(2,128)} %squeeze.586) | copy-start | bytes 1540
  269.7 27.4 %copy-start.55 = (f32[2,64]{1,0:T(2,128)S(1)}, f32[2,64]{1,0:T(2,128)}, u32[]{:S(2)}) copy-start(f32[2,64]{1,0:T(2,128)} %squeeze.585) | copy-start | bytes 1540
  269.8 27.4 %copy-start.56 = (f32[2,64]{1,0:T(2,128)S(1)}, f32[2,64]{1,0:T(2,128)}, u32[]{:S(2)}) copy-start(f32[2,64]{1,0:T(2,128)} %squeeze.584) | copy-start | bytes 1540
  313.0 15.1 %all-to-all-start.3 = ((bf16[4,192,512]{2,1,0:T(8,128)(2,1)}), bf16[4,192,512]{2,1,0:T(8,128)(2,1)S(1)}, u32[]{:S(2)}, u32[]{:S(2)}) async-start(bf16[4,192,512]{2,1,0:T(8,128)(2,1)} %stack.2), calls=%async_computation.4 | async-start | bytes 1572864 | tf_op jit(solution)/shard_map/all_to_all | solution.py:261
  336.7 39.4 %copy-start.8 = (f32[2,256,64]{1,2,0:T(8,128)S(1)}, f32[2,256,64]{1,2,0:T(8,128)}, u32[]{:S(2)}) copy-start(f32[2,256,64]{1,2,0:T(8,128)} %reverse.7) | copy-start | bytes 393220
  336.9 39.4 %copy-start.4 = (bf16[2,192,128]{2,1,0:T(8,128)(2,1)}, bf16[2,192,128]{2,1,0:T(8,128)(2,1)S(1)}, u32[]{:S(2)}) copy-start(bf16[2,192,128]{2,1,0:T(8,128)(2,1)S(1)} %add_add_fusion) | copy-start | bytes 294916
  336.9 39.4 %copy-start.61 = (f32[1,128]{1,0:T(1,128)S(1)}, f32[1,128]{1,0:T(1,128)}, u32[]{:S(2)}) copy-start(f32[1,128]{1,0:T(1,128)} %copy-done.60) | copy-start | bytes 1540
  376.4 44.5 %copy-start.5 = (bf16[2,192,128]{2,1,0:T(8,128)(2,1)S(1)}, bf16[2,192,128]{2,1,0:T(8,128)(2,1)}, u32[]{:S(2)}) copy-start(bf16[2,192,128]{2,1,0:T(8,128)(2,1)} %copy-done.4) | copy-start | bytes 294916
  428.9 94.5 %all-to-all-start.4 = ((f32[64,32,256]{2,1,0:T(8,128)}), f32[64,32,256]{2,1,0:T(8,128)}, u32[]{:S(2)}, u32[]{:S(2)}) async-start(f32[64,32,256]{2,1,0:T(8,128)} %fusion.250), calls=%async_computation.5 | async-start | bytes 4194304 | tf_op jit(solution)/shard_map/all_to_all | solution.py:93
  485.0 33.0 %copy-start.9 = (f32[2,256,64]{1,2,0:T(8,128)S(1)}, f32[2,256,64]{1,2,0:T(8,128)}, u32[]{:S(2)}) copy-start(f32[2,256,64]{1,2,0:T(8,128)} %reverse.7) | copy-start | bytes 393220
  485.0 33.0 %copy-start.38 = (bf16[2,64,128]{2,1,0:T(8,128)(2,1)S(1)}, bf16[2,64,128]{2,1,0:T(8,128)(2,1)}, u32[]{:S(2)}) copy-start(bf16[2,64,128]{2,1,0:T(8,128)(2,1)} %add_add_fusion.3) | copy-start | bytes 98308
  485.0 33.2 %copy-start.13 = (f32[2,256,64]{1,2,0:T(8,128)S(1)}, f32[2,256,64]{1,2,0:T(8,128)}, u32[]{:S(2)}) copy-start(f32[2,256,64]{1,2,0:T(8,128)} %bitcast_bitcast_fusion.1) | copy-start | bytes 393220
  (77 other events, 1191.4 us)
Sparse Core Ops, SparseCore 0:
  146.8 34.0 reduce-scatter.1
